TPU v7x, 32 devices: a whole 2x2x4 slice. The times are simulated.
32 devices in a mesh: sp: 4 (over z), fs: 4 (over y, x), tp: 2 (over core).
Axes of the slice: x: 2, y: 2, z: 4, core: 2. Of those that a mesh axis runs over, the one named last changes fastest.
Arguments:
- tokens: bfloat16 [4, 1024, 2048], P('fs', 'sp', 'tp'), may hold values from -6 to 6
- norm_gain: float32 [2048], replicated, may hold values from 0.1 to 1.9
- ret_query: bfloat16 [2048, 1024], P('sp', 'tp'), may hold values from -0.125 to 0.125
- ret_key: bfloat16 [2048, 1024], P('sp', 'tp'), may hold values from -0.125 to 0.125
- ret_value: bfloat16 [2048, 1024], P('sp', 'tp'), may hold values from -0.125 to 0.125
- att_query: bfloat16 [2048, 1024], P('sp', 'tp'), may hold values from -0.125 to 0.125
- att_key: bfloat16 [2048, 256], P('sp', 'tp'), may hold values from -0.125 to 0.125
- att_value: bfloat16 [2048, 256], P('sp', 'tp'), may hold values from -0.125 to 0.125
- log_decay: float32 [4, 4, 1024], P('fs', 'tp', 'sp'), may hold values from -1 to 0
- start_state: float32 [4, 4, 256, 256], P('fs', 'tp'), may hold values from -12 to 12
- ret_gain: float32 [1024], P('tp'), may hold values from 0.1 to 1.9
- sink_logits: float32 [16], P('tp'), may hold values from 1 to 5
- ret_out: bfloat16 [1024, 2048], P('tp', 'fs'), may hold values from -0.1875 to 0.1875
- att_out: bfloat16 [1024, 2048], P('tp', 'fs'), may hold values from -1.5 to 1.5
Outputs:
- mixed: bfloat16 [4, 1024, 2048], P('fs', 'sp', 'tp')
All inputs are finite; a program needn't handle non-finite values.
Results may differ from a plain program's by a relative error of at most 0.015.
Values may be sent and summed in bfloat16 or wider, within the bound.
A program may use at most 128 MiB of HBM per device.

v0:
```python
import jax
import jax.numpy as jnp
from jax import lax
from jax.sharding import PartitionSpec as P

DK = 256
DV = 256
HD = 64
WINDOW = 128
BLOCK = 128
epsilon = 1e-06
exact_result = lax.Precision.HIGHEST


def carried_in(array, axis, combine, identity):
    peers, mine = (lax.axis_size(axis), lax.axis_index(axis))
    everything = jax.tree.map(
        lambda part, kind: lax.all_gather(part.astype(kind), axis),
        array,
        (jnp.bfloat16, jnp.bfloat16),
    )
    start = jax.tree.map(
        lambda part, zero: jnp.broadcast_to(jnp.asarray(zero, part.dtype), part.shape),
        array,
        identity,
    )

    def hop(k, before):
        reached = k < mine
        new = combine(
            before, jax.tree.map(lambda part, own: part[k].astype(own.dtype), everything, array)
        )
        return jax.tree.map(lambda a, b: jnp.where(reached, a, b), new, before)

    return lax.fori_loop(0, peers, hop, start)


def passed_along(block, axis, distance):
    devices = range(lax.axis_size(axis))
    route = [(i - distance, i) for i in devices if i - distance in devices]
    return lax.ppermute(block, axis, route)


def rotate(values, positions):
    half_dim = values.shape[-1] // 2
    inverse = 1.0 / 10000.0 ** (jnp.arange(half_dim, dtype=jnp.float32) / half_dim)
    angles = positions.astype(jnp.float32)[:, None] * inverse[None, :]
    cosine = jnp.cos(angles)[:, None, :]
    sine_table = jnp.sin(angles)[:, None, :]
    front_half = values[..., :half_dim]
    back_half = values[..., half_dim:]
    return jnp.concatenate(
        [
            front_half * cosine - back_half * sine_table,
            front_half * sine_table + back_half * cosine,
        ],
        axis=-1,
    )


def block_step(memory_state, inputs):
    queries, key_matrix_rows, value_matrix_rows, log_rates = inputs
    length_here = log_rates.shape[-1]
    causal = jnp.arange(length_here)[:, None] >= jnp.arange(length_here)[None, :]
    running_totals = jnp.cumsum(log_rates, axis=-1)
    relative = running_totals[:, :, None] - running_totals[:, None, :]
    weight = jnp.where(causal[None], jnp.exp(jnp.where(causal[None], relative, 0.0)), 0.0)
    score_matrix = (
        jnp.einsum("hqd,hkd->hqk", queries, key_matrix_rows, precision=exact_result) * weight
    )
    carried_state = jnp.einsum(
        "hqd,hdv->hqv",
        queries * jnp.exp(running_totals)[:, :, None],
        memory_state,
        precision=exact_result,
    )
    output_rows = (
        jnp.einsum("arf,afu->aru", score_matrix, value_matrix_rows, precision=exact_result)
        + carried_state
    )
    decay_factors = jnp.exp(running_totals[:, -1:] - running_totals)
    memory_state = memory_state * jnp.exp(running_totals[:, -1])[:, None, None] + jnp.einsum(
        "iwj,iwe->ije",
        key_matrix_rows * decay_factors[:, :, None],
        value_matrix_rows,
        precision=exact_result,
    )
    return (memory_state, output_rows)


def chain(earlier, later):
    return (earlier[0] * later[0], earlier[1] * later[0][:, None, None] + later[1])


def shards(
    tokens,
    norm_gain,
    ret_query,
    ret_key,
    ret_value,
    att_query,
    att_key,
    att_value,
    log_decay,
    start_state,
    ret_gain,
    sink_logits,
    ret_out,
    att_out,
):
    gathered = lax.all_gather(tokens[0], "tp", axis=1, tiled=True)
    row_count = gathered.shape[0]
    as_float = gathered.astype(jnp.float32)
    normed = (
        as_float
        * lax.rsqrt(jnp.mean(as_float * as_float, axis=-1, keepdims=True) + epsilon)
        * norm_gain
    ).astype(jnp.bfloat16)
    offset = lax.axis_index("sp") * row_count
    positions = offset + jnp.arange(row_count, dtype=jnp.int32)
    weights = (ret_query, ret_key, ret_value, att_query, att_key, att_value)
    pieces = (
        lax.all_gather(weights[0], "sp", axis=0, tiled=True),
        lax.all_gather(weights[1], "sp", axis=0, tiled=True),
        lax.all_gather(weights[2], "sp", axis=0, tiled=True),
        lax.all_gather(weights[3], "sp", axis=0, tiled=True),
        lax.all_gather(weights[4], "sp", axis=0, tiled=True),
        lax.all_gather(weights[5], "sp", axis=0, tiled=True),
    )
    projected = tuple(
        (jnp.dot(normed, piece, preferred_element_type=jnp.float32) for piece in pieces)
    )
    rounded = tuple((product_f.astype(jnp.bfloat16) for product_f in projected))
    projected = rounded[:3]
    head_count = projected[0].shape[1] // DK
    queries = rotate(projected[0].astype(jnp.float32).reshape(row_count, head_count, DK), positions)
    keys_rot = rotate(
        projected[1].astype(jnp.float32).reshape(row_count, head_count, DK), positions
    ) * DK ** (-0.5)
    values_f = projected[2].astype(jnp.float32).reshape(row_count, head_count, DV)
    log_rates = log_decay[0]
    count = row_count // BLOCK

    def blocked(array):
        return array.reshape(count, BLOCK, head_count, array.shape[-1]).transpose(0, 2, 1, 3)

    rates_blocked = log_rates.reshape(head_count, count, BLOCK).transpose(1, 0, 2)
    local_state, pieces = lax.scan(
        block_step,
        jnp.zeros((head_count, DK, DV), jnp.float32),
        (blocked(queries), blocked(keys_rot), blocked(values_f), rates_blocked),
    )
    local_out = pieces.transpose(0, 2, 1, 3).reshape(row_count, head_count, DV)
    running_totals = jnp.cumsum(log_rates, axis=-1)
    device_decay = jnp.exp(running_totals[:, -1])
    identity = (jnp.ones((head_count,), jnp.float32), jnp.zeros((head_count, DK, DV), jnp.float32))
    prior_decay, prior_state = carried_in((device_decay, local_state), "sp", chain, identity)
    incoming = prior_state + prior_decay[:, None, None] * start_state[0]
    retained = local_out + jnp.einsum(
        "thd,hdv->thv",
        queries * jnp.exp(running_totals).T[:, :, None],
        incoming,
        precision=exact_result,
    )
    centred = retained - jnp.mean(retained, axis=-1, keepdims=True)
    variance = jnp.mean(centred * centred, axis=-1, keepdims=True)
    ret_hidden = (
        (centred * lax.rsqrt(variance + epsilon)).reshape(row_count, head_count * DV) * ret_gain
    ).astype(jnp.bfloat16)
    att_queries, att_keys, att_values = rounded[3:]
    kv_heads = att_keys.shape[1] // HD
    groups = att_queries.shape[1] // HD // kv_heads
    earlier_keys, earlier_values = passed_along(
        (att_keys[row_count - WINDOW :], att_values[row_count - WINDOW :]), "sp", 1
    )
    extended_keys = jnp.concatenate([earlier_keys, att_keys], axis=0)
    extended_values = jnp.concatenate([earlier_values, att_values], axis=0)
    windows = row_count // WINDOW

    def banded(array):
        earlier = array[:row_count].reshape(windows, WINDOW, kv_heads, HD)
        current = array[WINDOW:].reshape(windows, WINDOW, kv_heads, HD)
        return jnp.concatenate([earlier, current], axis=1)

    key_band = banded(extended_keys)
    value_band = banded(extended_values)
    grouped_q = att_queries.reshape(windows, WINDOW, kv_heads, groups, HD)
    score_matrix = jnp.einsum(
        "nqhgd,nkhd->nhgqk", grouped_q, key_band, preferred_element_type=jnp.float32
    ) * HD ** (-0.5)
    query_index = WINDOW + jnp.arange(WINDOW)
    key_index = jnp.arange(2 * WINDOW)
    allowed = (key_index[None, :] <= query_index[:, None]) & (
        query_index[:, None] - key_index[None, :] < WINDOW
    )
    key_place = offset - WINDOW + jnp.arange(windows)[:, None] * WINDOW + key_index[None, :]
    visible = (allowed[None] & (key_place >= 0)[:, None, :])[:, None, None]
    expo = jnp.exp(jnp.where(visible, score_matrix, -1e30))
    summed = jnp.sum(expo, axis=-1, keepdims=True) + jnp.exp(sink_logits).reshape(
        1, kv_heads, groups, 1, 1
    )
    probs = (expo / summed).astype(jnp.bfloat16)
    attended = jnp.einsum(
        "nhgqk,nkhd->nqhgd", probs, value_band, preferred_element_type=jnp.float32
    )
    att_hidden = attended.astype(jnp.bfloat16).reshape(row_count, kv_heads * groups * HD)
    ret_width = ret_hidden.shape[1]
    joined = jnp.concatenate([ret_hidden, att_hidden], axis=1)[None]
    piece = lax.all_gather(joined, "fs", axis=0, tiled=True)
    product = jnp.einsum(
        "srh,hd->srd", piece[:, :, :ret_width], ret_out, preferred_element_type=jnp.float32
    )
    product = product + jnp.einsum(
        "srh,hd->srd", piece[:, :, ret_width:], att_out, preferred_element_type=jnp.float32
    )
    partial_rows = product.astype(jnp.bfloat16)
    regrouped = lax.all_to_all(partial_rows, "fs", split_axis=0, concat_axis=2, tiled=True)
    mixed = lax.psum_scatter(
        regrouped[0].astype(jnp.float32).astype(jnp.bfloat16), "tp", scatter_dimension=1, tiled=True
    )
    return mixed[None]


def solution(mesh):
    placed = (
        P("fs", "sp", "tp"),
        P(),
        P("sp", "tp"),
        P("sp", "tp"),
        P("sp", "tp"),
        P("sp", "tp"),
        P("sp", "tp"),
        P("sp", "tp"),
        P("fs", "tp", "sp"),
        P("fs", "tp", None, None),
        P("tp"),
        P("tp"),
        P("tp", "fs"),
        P("tp", "fs"),
    )
    return jax.shard_map(
        shards, mesh=mesh, in_specs=placed, out_specs=P("fs", "sp", "tp"), check_vma=False
    )
```

profile of v0, /device:TPU:0, one launch (start us, length us, event | category | flops | bytes accessed | tf_op | source)
XLA Modules:
  0.0 330.0 jit_solution(6295431087866726067)
XLA Ops:
  13.0 13.6 %all-reduce = bf16[8]{0:T(256)(128)(2,1)S(1)} all-reduce(bf16[8]{0:T(256)(128)(2,1)S(1)} %dynamic-update-slice), channel_id=3, replica_groups=mesh['sp'=4,'fs'=4,'tp'=2] {'sp'}, use_global_device_ids=true, to_apply=%add | all-reduce | flops 8 | bytes 32
  26.6 18.4 %all_gather.42 = bf16[2048,128]{1,0:T(8,128)(2,1)S(1)} all-gather(bf16[512,128]{1,0:T(8,128)(2,1)S(1)} %copy-done.12), channel_id=1, replica_groups=mesh['sp'=4,'fs'=4,'tp'=2] {'sp'}, dimensions={0}, use_global_device_ids=true | all-gather | bytes 655360 | tf_op jit(solution)/shard_map/all_gather | solution.py:127
  45.7 21.2 %all_gather.41 = bf16[2048,128]{1,0:T(8,128)(2,1)} all-gather(bf16[512,128]{1,0:T(8,128)(2,1)S(1)} %copy-done.13), channel_id=1, replica_groups=mesh['sp'=4,'fs'=4,'tp'=2] {'sp'}, dimensions={0}, use_global_device_ids=true | all-gather | bytes 655360 | tf_op jit(solution)/shard_map/all_gather | solution.py:128
  68.9 1.6 fusion.25
  70.5 1.7 convolution_convert_fusion.5
  72.9 2.6 collective-permute-start.1
  75.5 5.5 %all-gather.12.cloned.1.call-done = bf16[2048,512]{1,0:T(8,128)(2,1)} async-done(((bf16[512,512]{1,0:T(8,128)(2,1)}), bf16[2048,512]{1,0:T(8,128)(2,1)}) %all-gather.12.cloned.1.call-update) | async-done | bytes 2097168 | tf_op jit(solution)/shard_map/all_gather | solution.py:124
  80.9 2.3 fusion.31
  83.6 44.0 %all-gather.16.cloned.1.call-done = bf16[2048,512]{1,0:T(8,128)(2,1)} async-done(((bf16[512,512]{1,0:T(8,128)(2,1)}), bf16[2048,512]{1,0:T(8,128)(2,1)}) %all-gather.16.cloned.1.call-update) | async-done | bytes 2097168 | tf_op jit(solution)/shard_map/all_gather | solution.py:123
  127.6 2.7 fusion.33
  131.4 42.1 %all-gather.14.cloned.1.call-done = bf16[2048,512]{1,0:T(8,128)(2,1)} async-done(((bf16[512,512]{1,0:T(8,128)(2,1)}), bf16[2048,512]{1,0:T(8,128)(2,1)}) %all-gather.14.cloned.1.call-update) | async-done | bytes 2097168 | tf_op jit(solution)/shard_map/all_gather | solution.py:125
  173.6 2.7 fusion.32
  178.9 6.7 %while.29 = (s32[]{:T(128)}, f32[2,256,256]{2,1,0:T(8,128)S(1)}, f32[2,2,128,256]{3,2,1,0:T(8,128)}, f32[2,2,128]{2,1,0:T(2,128)S(1)}, f32[2,2,128,256]{3,2,0,1:...) while((s32[]{:T(128)}, f32[2,256,256]{2,1,0:T(8,128)S(1)}, ...), condition=%wide.region_3.4_spmd.clone, body=%wide.region_1.3_spmd.clone.sunk | while | flops 604880896 | bytes 4242084 | solution.py:148
  186.4 1.9 convolution_convert_fusion.6
  188.6 2.3 collective-permute-start
  194.9 24.5 %all-gather.18.cloned.1.call-done = bf16[2048,512]{1,0:T(8,128)(2,1)} async-done(((bf16[512,512]{1,0:T(8,128)(2,1)}), bf16[2048,512]{1,0:T(8,128)(2,1)}) %all-gather.18.cloned.1.call-update) | async-done | bytes 2097168 | tf_op jit(solution)/shard_map/all_gather | solution.py:126
  219.5 2.3 convolution_convert_fusion.1
  223.8 25.1 %all-gather.22.cloned.1.call-done = bf16[8,256,256]{2,1,0:T(8,128)(2,1)} async-done(((bf16[2,256,256]{2,1,0:T(8,128)(2,1)}), bf16[8,256,256]{2,1,0:T(8,128)(2,1)}) %all-gather.22.cloned.1.call-update) | async-done | bytes 1048592 | tf_op jit(solution)/shard_map/all_gather | solution.py:18
  248.9 4.6 %while.30 = (s32[]{:T(128)}, f32[2]{0:T(128)S(1)}, f32[2,256,256]{2,1,0:T(8,128)S(1)}, s32[]{:T(128)}, bf16[4,2]{1,0:T(4,128)(2,1)S(1)}, /*index=5*/bf16[4,2,256,256]{3,2,1,0:T(8,128)(2,1)}, s32[]{:T(128)}, s32[]{:T(128)}) while((s32[]{:T(128)}, f32[2]{0:T(128)S(1)}, f32[2,256,256]{2,1,0:T(8,128)S(1)}, s32[]{:T(128)}, ...), condition=%wide.region_7.8_spmd.clone, body=%wide.region_6.7_spmd.clone.sunk | while | flops 655372 | bytes 1310871 | solution.py:35
  255.9 34.5 %all-gather.24.cloned.1.call-done = bf16[1024,1024]{0,1:T(8,128)(2,1)} async-done(((bf16[256,1024]{0,1:T(8,128)(2,1)}), bf16[1024,1024]{0,1:T(8,128)(2,1)}) %all-gather.24.cloned.1.call-update) | async-done | bytes 2097168 | tf_op jit(solution)/shard_map/all_gather | solution.py:209
  290.4 2.9 copy.81
  295.1 16.7 %all_to_all.15 = bf16[4,256,512]{2,1,0:T(8,128)(2,1)S(1)} all-to-all(bf16[4,256,512]{2,1,0:T(8,128)(2,1)S(1)} %add_convert_fusion), channel_id=1, replica_groups=mesh['sp'=4,'fs'=4,'tp'=2] {'fs'}, dimensions={0} | all-to-all | bytes 2097152 | tf_op jit(solution)/shard_map/all_to_all | solution.py:217
  313.1 8.0 %reduce-scatter.2.cloned.1.call-done = bf16[256,1024]{0,1:T(8,128)(2,1)} async-done(((bf16[256,2048]{0,1:T(8,128)(2,1)}), bf16[256,1024]{0,1:T(8,128)(2,1)}) %reduce-scatter.2.cloned.1.call-update) | async-done | bytes 524304 | tf_op jit(solution)/shard_map/reduce_scatter | solution.py:218
  321.1 2.0 copy.83
  (162 shorter events, 36.5 us)
Async XLA Ops:
  6.5 286.8 %copy-start = (bf16[512,512]{1,0:T(8,128)(2,1)S(1)}, bf16[512,512]{1,0:T(8,128)(2,1)}, u32[]{:S(2)}) copy-start(bf16[512,512]{1,0:T(8,128)(2,1)} %param.30) | copy-start | bytes 1572868
  6.5 4.8 %copy-start.23 = (u32[32]{0:T(128)S(1)}, u32[32]{0:T(128)}, u32[]{:S(2)}) copy-start(u32[32]{0:T(128)} %constant.93) | copy-start | bytes 388
  6.5 20.1 %copy-start.12 = (bf16[512,128]{1,0:T(8,128)(2,1)S(1)}, bf16[512,128]{1,0:T(8,128)(2,1)}, u32[]{:S(2)}) copy-start(bf16[512,128]{1,0:T(8,128)(2,1)} %param.24) | copy-start | bytes 393220
  6.5 38.6 %copy-start.22 = (f32[8]{0:T(128)S(1)}, f32[8]{0:T(128)}, u32[]{:S(2)}) copy-start(f32[8]{0:T(128)} %param.29) | copy-start | bytes 100
  6.5 39.2 %copy-start.13 = (bf16[512,128]{1,0:T(8,128)(2,1)S(1)}, bf16[512,128]{1,0:T(8,128)(2,1)}, u32[]{:S(2)}) copy-start(bf16[512,128]{1,0:T(8,128)(2,1)} %param.25) | copy-start | bytes 393220
  6.6 62.3 %all-gather.20.cloned.1.call-start = ((), (), s32[]{:S(2)}) async-start(), calls=%async_computation.7 | async-start | bytes 1572864 | tf_op jit(solution)/shard_map/all_gather | solution.py:111
  7.3 73.6 %all-gather.12.cloned.1.call-start = ((), (), s32[]{:S(2)}) async-start(), calls=%async_computation.2 | async-start | bytes 2621440 | tf_op jit(solution)/shard_map/all_gather | solution.py:124
  8.0 62.5 %copy-start.20 = (f32[2048]{0:T(1024)S(1)}, f32[2048]{0:T(1024)}, u32[]{:S(2)}) copy-start(f32[2048]{0:T(1024)} %param.19) | copy-start | bytes 24580
  8.1 119.6 %all-gather.16.cloned.1.call-start = ((), (), s32[]{:S(2)}) async-start(), calls=%async_computation.4 | async-start | bytes 2621440 | tf_op jit(solution)/shard_map/all_gather | solution.py:123
  8.8 164.8 %all-gather.14.cloned.1.call-start = ((), (), s32[]{:S(2)}) async-start(), calls=%async_computation.3 | async-start | bytes 2621440 | tf_op jit(solution)/shard_map/all_gather | solution.py:125
  9.4 210.1 %all-gather.18.cloned.1.call-start = ((), (), s32[]{:S(2)}) async-start(), calls=%async_computation.5 | async-start | bytes 2621440 | tf_op jit(solution)/shard_map/all_gather | solution.py:126
  10.0 238.9 %all-gather.22.cloned.1.call-start = ((), (), s32[]{:S(2)}) async-start(), calls=%async_computation.8 | async-start | bytes 1310720 | tf_op jit(solution)/shard_map/all_gather | solution.py:18
  68.9 12.1 %copy-start.5 = (bf16[1,256,2048]{2,1,0:T(8,128)(2,1)S(1)}, bf16[1,256,2048]{2,1,0:T(8,128)(2,1)}, u32[]{:S(2)}) copy-start(bf16[1,256,2048]{2,1,0:T(8,128)(2,1)} %all-gather.20.cloned.1.call-done) | copy-start | bytes 3145732
  70.5 103.1 %copy-start.18 = (f32[256]{0:T(256)}, f32[256]{0:T(256)S(1)}, u32[]{:S(2)}) copy-start(f32[256]{0:T(256)S(1)} %add_rsqrt_fusion.1) | copy-start | bytes 3076
  72.2 11.0 %copy-start.10 = (bf16[256,128]{1,0:T(8,128)(2,1)}, bf16[256,128]{1,0:T(8,128)(2,1)S(1)}, u32[]{:S(2)}) copy-start(bf16[256,128]{1,0:T(8,128)(2,1)S(1)} %convolution_convert_fusion.5) | copy-start | bytes 196612
  72.9 118.2 %collective-permute-start.1 = (bf16[128,128]{1,0:T(8,128)(2,1)}, bf16[128,128]{1,0:T(8,128)(2,1)}, u32[]{:S(2)}, u32[]{:S(2)}) collective-permute-start(bf16[128,128]{1,0:T(8,128)(2,1)} %slice.64), channel_id=1, source_target_pairs={{0,8},{8,16},{16,24},{1,9},{9,17},{17,25},{2,10},{10,18},{18,26},{... | collective-permute-start | bytes 98312 | tf_op jit(solution)/shard_map/ppermute | solution.py:41
  178.8 7.6 %copy-start.19 = (f32[256]{0:T(256)S(1)}, f32[256]{0:T(256)}, u32[]{:S(2)}) copy-start(f32[256]{0:T(256)} %copy-done.18) | copy-start | bytes 3076
  178.8 7.6 %copy-start.21 = (f32[2048]{0:T(1024)S(1)}, f32[2048]{0:T(1024)}, u32[]{:S(2)}) copy-start(f32[2048]{0:T(1024)} %param.19) | copy-start | bytes 24580
  186.4 104.1 %all-gather.24.cloned.1.call-start = ((), (), s32[]{:S(2)}) async-start(), calls=%async_computation.9 | async-start | bytes 2621440 | tf_op jit(solution)/shard_map/all_gather | solution.py:209
  188.3 31.2 %copy-start.6 = (bf16[1,256,2048]{2,1,0:T(8,128)(2,1)S(1)}, bf16[1,256,2048]{2,1,0:T(8,128)(2,1)}, u32[]{:S(2)}) copy-start(bf16[1,256,2048]{2,1,0:T(8,128)(2,1)} %all-gather.20.cloned.1.call-done) | copy-start | bytes 3145732
  188.6 4.3 %collective-permute-start = (bf16[128,128]{1,0:T(8,128)(2,1)S(1)}, bf16[128,128]{1,0:T(8,128)(2,1)S(1)}, u32[]{:S(2)}, u32[]{:S(2)}) collective-permute-start(bf16[128,128]{1,0:T(8,128)(2,1)S(1)} %slice.63), channel_id=1, source_target_pairs={{0,8},{8,16},{16,24},{1,9},{9,17},{17,25},{2,10},{10,18},{18,26},{... | collective-permute-start | bytes 98312 | tf_op jit(solution)/shard_map/ppermute | solution.py:41
  194.9 27.2 %copy-start.14 = (pred[2,128,256]{1,2,0:T(8,128)(4,1)S(1)}, pred[2,128,256]{1,2,0:T(8,128)(4,1)}, u32[]{:S(2)}) copy-start(pred[2,128,256]{1,2,0:T(8,128)(4,1)} %broadcast_and_fusion) | copy-start | bytes 196612
  248.9 4.6 %copy-start.9 = (f32[1,2,256,256]{3,2,1,0:T(8,128)S(1)}, f32[1,2,256,256]{3,2,1,0:T(8,128)}, u32[]{:S(2)}) copy-start(f32[1,2,256,256]{3,2,1,0:T(8,128)} %param.27) | copy-start | bytes 1572868
  255.9 65.2 %reduce-scatter.2.cloned.1.call-start = ((), (), s32[]{:S(2)}) async-start(), calls=%async_computation.6 | async-start | bytes 1572864 | tf_op jit(solution)/shard_map/reduce_scatter | solution.py:218
  (10 other events, 21.6 us)
Sparse Core Ops, SparseCore 0:
  8.9 11.7 all-gather.19
  22.3 58.6 all-gather.11
  82.5 45.0 all-gather.15
  129.1 44.4 all-gather.13
  175.0 44.4 all-gather.17
  220.9 27.9 all-gather.21
  256.0 34.4 all-gather.23
  313.2 7.8 reduce-scatter.1
where the time goes:
time: 331 us; the launch traced here: 330 us
  waiting for transfers between devices  188 us (57%)
  blocking collectives  69.8 us (21%)
  matrix products  23 us (7%)
  local copies, waits for them, and re-layouts  16.4 us (5%)
  between operations  14.8 us (4%)
  other arithmetic  12.8 us (4%)
  starting transfers between devices  5.19 us (2%)
    all_gather x1, waiting for transfers between devices, shards(): lax.all_gather(weights[0], 'sp', axis=0, tiled=True)  44 us
    all_gather x1, waiting for transfers between devices, shards(): lax.all_gather(weights[2], 'sp', axis=0, tiled=True)  42.1 us
    all_gather x1, waiting for transfers between devices, shards(): piece = lax.all_gather(joined, 'fs', axis=0, tiled=True)  34.5 us
    all_gather x1, waiting for transfers between devices, carried_in(): lax.all_gather(part.astype(kind), axis)  25.1 us
    all_gather x1, waiting for transfers between devices, shards(): lax.all_gather(weights[3], 'sp', axis=0, tiled=True)  24.5 us
    all_gather x1, blocking collectives, shards(): lax.all_gather(weights[5], 'sp', axis=0, tiled=True)  21.2 us
    all_gather x1, blocking collectives, shards(): lax.all_gather(weights[4], 'sp', axis=0, tiled=True)  18.4 us
    all_to_all x1, blocking collectives, shards(): lax.all_to_all(partial_rows, 'fs', split_axis=0, concat_axis=2, tiled=True)  16.7 us
  transfers between devices with their start and end apart: 10, of which 8 were waited for; matrix products, arithmetic and copies ran while one was open for 11% of the time, Pallas kernels for 0%

commit v1 on v0

--- a/solution.py
+++ b/solution.py
@@ -10,6 +10,19 @@
 BLOCK = 128
 epsilon = 1e-06
 exact_result = lax.Precision.HIGHEST
+
+
+def collect(x, axis, dim):
+    size, index, span = (lax.axis_size(axis), lax.axis_index(axis), x.shape[dim])
+    right = [(i, (i + 1) % size) for i in range(size)]
+    out = jnp.zeros((*x.shape[:dim], size * span, *x.shape[dim + 1 :]), x.dtype)
+    held = x
+    for hop in range(size):
+        source = (index - hop) % size
+        out = lax.dynamic_update_slice_in_dim(out, held, source * span, axis=dim)
+        if hop < size - 1:
+            held = lax.ppermute(held, axis, right)
+    return out
 
 
 def carried_in(array, axis, combine, identity):
@@ -123,7 +136,7 @@
         lax.all_gather(weights[0], "sp", axis=0, tiled=True),
         lax.all_gather(weights[1], "sp", axis=0, tiled=True),
         lax.all_gather(weights[2], "sp", axis=0, tiled=True),
-        lax.all_gather(weights[3], "sp", axis=0, tiled=True),
+        collect(weights[3], "sp", 0),
         lax.all_gather(weights[4], "sp", axis=0, tiled=True),
         lax.all_gather(weights[5], "sp", axis=0, tiled=True),
     )

time: 331 us -> 315 us (0.952)
  waiting for transfers between devices: 188 us -> 144 us
  local copies, waits for them, and re-layouts: 16.4 us -> 32 us
  starting transfers between devices: 5.19 us -> 11.8 us
  blocking collectives: 69.8 us -> 73.6 us
    all_gather x1 -> x0, waiting for transfers between devices: 24.5 us -> none  [shards(): lax.all_gather(weights[3], 'sp', axis=0, tiled=True)]
    all_gather x1, waiting for transfers between devices: 25.1 us -> 17.6 us  [carried_in(): lax.all_gather(part.astype(kind), axis)]
    dynamic_update_slice x0 -> x4, local copies, waits for them, and re-layouts: none -> 6.6 us  [collect(): out = lax.dynamic_update_slice_in_dim(out, held, source * span, axis=dim)]
    all_gather x1, waiting for transfers between devices: 5.46 us -> 0.01 us  [shards(): lax.all_gather(weights[1], 'sp', axis=0, tiled=True)]
    ppermute x0 -> x3, starting transfers between devices: none -> 4.12 us  [collect(): held = lax.ppermute(held, axis, right)]
  transfers between devices with their start and end apart: 10 -> 12, of which waited for: 8 -> 6; matrix products, arithmetic and copies ran while one was open for 11% -> 17% of each run, Pallas kernels for 0% -> 0%
where the time goes in v1:
time: 315 us; the launch traced here: 314 us
  waiting for transfers between devices  144 us (46%)
  blocking collectives  73.6 us (23%)
  local copies, waits for them, and re-layouts  32 us (10%)
  matrix products  24.4 us (8%)
  between operations  14.9 us (5%)
  other arithmetic  13.6 us (4%)
  starting transfers between devices  11.8 us (4%)
    all_gather x1, waiting for transfers between devices, shards(): lax.all_gather(weights[0], 'sp', axis=0, tiled=True)  40.8 us
    all_gather x1, waiting for transfers between devices, shards(): lax.all_gather(weights[2], 'sp', axis=0, tiled=True)  39.8 us
    all_gather x1, waiting for transfers between devices, shards(): piece = lax.all_gather(joined, 'fs', axis=0, tiled=True)  34.5 us
    all_gather x1, blocking collectives, shards(): lax.all_gather(weights[5], 'sp', axis=0, tiled=True)  22.2 us
    all_gather x1, blocking collectives, shards(): lax.all_gather(weights[4], 'sp', axis=0, tiled=True)  19.9 us
    all_gather x1, waiting for transfers between devices, carried_in(): lax.all_gather(part.astype(kind), axis)  17.6 us
    all_to_all x1, blocking collectives, shards(): lax.all_to_all(partial_rows, 'fs', split_axis=0, concat_axis=2, tiled=True)  16.7 us
    dot_general x6, matrix products, shards(): jnp.dot(normed, piece, preferred_element_type=jnp.float32)  15.1 us
  transfers between devices with their start and end apart: 12, of which 6 were waited for; matrix products, arithmetic and copies ran while one was open for 17% of the time, Pallas kernels for 0%

profile of v1, /device:TPU:0, one launch (start us, length us, event | category | flops | bytes accessed | tf_op | source)
XLA Modules:
  0.0 313.8 jit_solution(5642508713859263436)
XLA Ops:
  8.8 3.1 collective-permute-start.2
  14.9 14.8 %all-reduce = bf16[8]{0:T(256)(128)(2,1)S(1)} all-reduce(bf16[8]{0:T(256)(128)(2,1)S(1)} %dynamic-update-slice), channel_id=3, replica_groups=mesh['sp'=4,'fs'=4,'tp'=2] {'sp'}, use_global_device_ids=true, to_apply=%add | all-reduce | flops 8 | bytes 32
  30.4 19.9 %all_gather.39 = bf16[2048,128]{1,0:T(8,128)(2,1)S(1)} all-gather(bf16[512,128]{1,0:T(8,128)(2,1)S(1)} %copy-done.16), channel_id=1, replica_groups=mesh['sp'=4,'fs'=4,'tp'=2] {'sp'}, dimensions={0}, use_global_device_ids=true | all-gather | bytes 655360 | tf_op jit(solution)/shard_map/all_gather | solution.py:140
  51.0 22.2 %all_gather.38 = bf16[2048,128]{1,0:T(8,128)(2,1)} all-gather(bf16[512,128]{1,0:T(8,128)(2,1)S(1)} %copy-done.17), channel_id=1, replica_groups=mesh['sp'=4,'fs'=4,'tp'=2] {'sp'}, dimensions={0}, use_global_device_ids=true | all-gather | bytes 655360 | tf_op jit(solution)/shard_map/all_gather | solution.py:141
  78.3 1.9 constant_dynamic-update-slice_fusion.2
  86.6 4.1 %collective-permute-start.1 = (bf16[128,128]{1,0:T(8,128)(2,1)}, bf16[128,128]{1,0:T(8,128)(2,1)}, u32[]{:S(2)}, u32[]{:S(2)}) collective-permute-start(bf16[128,128]{1,0:T(8,128)(2,1)} %slice.64), channel_id=1, source_target_pairs={{0,8},{8,16},{16,24},{1,9},{9,17},{17,25},{2,10},{10,18},{18,26},{... | collective-permute-start | bytes 98312 | tf_op jit(solution)/shard_map/ppermute | solution.py:54
  91.5 3.0 collective-permute-start
  96.9 1.9 constant_dynamic-update-slice_fusion.1
  98.8 3.1 fusion.31
  103.3 40.8 %all-gather.15.cloned.1.call-done = bf16[2048,512]{1,0:T(8,128)(2,1)} async-done(((bf16[512,512]{1,0:T(8,128)(2,1)}), bf16[2048,512]{1,0:T(8,128)(2,1)}) %all-gather.15.cloned.1.call-update) | async-done | bytes 2097168 | tf_op jit(solution)/shard_map/all_gather | solution.py:136
  144.1 3.1 %fusion.33 = f32[256,512]{1,0:T(8,128)} fusion(bf16[2048,512]{1,0:T(8,128)(2,1)} %all-gather.15.cloned.1.call-done, bf16[1,256,2048]{2,1,0:T(8,128)(2,1)S(1)} %copy-done.5, f32[2048]{0:T(1024)S(1)} %copy-done.32, f32[256]{0:T(256)S(1)} %add_rsqrt_fusion.1), kind=kOutput, calls=%fused_computation.57 | convolution fusion | flops 539230208 | bytes 3679232 | tf_op jit(solution)/shard_map/dot_general | solution.py:144
  147.3 2.2 reshape.299
  149.5 39.8 %all-gather.13.cloned.1.call-done = bf16[2048,512]{1,0:T(8,128)(2,1)} async-done(((bf16[512,512]{1,0:T(8,128)(2,1)}), bf16[2048,512]{1,0:T(8,128)(2,1)}) %all-gather.13.cloned.1.call-update) | async-done | bytes 2097168 | tf_op jit(solution)/shard_map/all_gather | solution.py:138
  189.3 3.1 fusion.32
  196.1 8.9 %while.29 = (s32[]{:T(128)}, f32[2,256,256]{2,1,0:T(8,128)S(1)}, f32[2,2,128,256]{3,2,1,0:T(8,128)}, f32[2,2,128]{2,1,0:T(2,128)S(1)}, f32[2,2,128,256]{3,2,0,1:...) while((s32[]{:T(128)}, f32[2,256,256]{2,1,0:T(8,128)S(1)}, ...), condition=%wide.region_3.4_spmd.clone, body=%wide.region_1.3_spmd.clone.sunk | while | flops 604880896 | bytes 4242144 | solution.py:161
  208.0 1.9 constant_dynamic-update-slice_fusion
  209.9 2.4 convolution_convert_fusion.1
  215.1 17.6 %all-gather.19.cloned.1.call-done = bf16[8,256,256]{2,1,0:T(8,128)(2,1)} async-done(((bf16[2,256,256]{2,1,0:T(8,128)(2,1)}), bf16[8,256,256]{2,1,0:T(8,128)(2,1)}) %all-gather.19.cloned.1.call-update) | async-done | bytes 1048592 | tf_op jit(solution)/shard_map/all_gather | solution.py:31
  232.7 4.6 %while.30 = (s32[]{:T(128)}, f32[2]{0:T(128)S(1)}, f32[2,256,256]{2,1,0:T(8,128)S(1)}, s32[]{:T(128)}, bf16[4,2]{1,0:T(4,128)(2,1)S(1)}, /*index=5*/bf16[4,2,256,256]{3,2,1,0:T(8,128)(2,1)}, s32[]{:T(128)}, s32[]{:T(128)}) while((s32[]{:T(128)}, f32[2]{0:T(128)S(1)}, f32[2,256,256]{2,1,0:T(8,128)S(1)}, s32[]{:T(128)}, ...), condition=%wide.region_7.8_spmd.clone, body=%wide.region_6.7_spmd.clone.sunk | while | flops 655372 | bytes 1310871 | solution.py:48
  239.8 34.5 %all-gather.21.cloned.1.call-done = bf16[1024,1024]{0,1:T(8,128)(2,1)} async-done(((bf16[256,1024]{0,1:T(8,128)(2,1)}), bf16[1024,1024]{0,1:T(8,128)(2,1)}) %all-gather.21.cloned.1.call-update) | async-done | bytes 2097168 | tf_op jit(solution)/shard_map/all_gather | solution.py:222
  274.3 2.9 copy.81
  279.0 16.7 %all_to_all.15 = bf16[4,256,512]{2,1,0:T(8,128)(2,1)S(1)} all-to-all(bf16[4,256,512]{2,1,0:T(8,128)(2,1)S(1)} %add_convert_fusion), channel_id=1, replica_groups=mesh['sp'=4,'fs'=4,'tp'=2] {'fs'}, dimensions={0} | all-to-all | bytes 2097152 | tf_op jit(solution)/shard_map/all_to_all | solution.py:230
  297.0 8.0 %reduce-scatter.2.cloned.1.call-done = bf16[256,1024]{0,1:T(8,128)(2,1)} async-done(((bf16[256,2048]{0,1:T(8,128)(2,1)}), bf16[256,1024]{0,1:T(8,128)(2,1)}) %reduce-scatter.2.cloned.1.call-update) | async-done | bytes 524304 | tf_op jit(solution)/shard_map/reduce_scatter | solution.py:231
  304.9 2.0 copy.83
  (196 shorter events, 49.5 us)
Async XLA Ops:
  6.5 270.6 %copy-start = (bf16[512,512]{1,0:T(8,128)(2,1)S(1)}, bf16[512,512]{1,0:T(8,128)(2,1)}, u32[]{:S(2)}) copy-start(bf16[512,512]{1,0:T(8,128)(2,1)} %param.30) | copy-start | bytes 1572868
  6.5 23.8 %copy-start.16 = (bf16[512,128]{1,0:T(8,128)(2,1)S(1)}, bf16[512,128]{1,0:T(8,128)(2,1)}, u32[]{:S(2)}) copy-start(bf16[512,128]{1,0:T(8,128)(2,1)} %param.24) | copy-start | bytes 393220
  6.5 43.8 %copy-start.34 = (f32[8]{0:T(128)S(1)}, f32[8]{0:T(128)}, u32[]{:S(2)}) copy-start(f32[8]{0:T(128)} %param.29) | copy-start | bytes 100
  6.5 44.4 %copy-start.17 = (bf16[512,128]{1,0:T(8,128)(2,1)S(1)}, bf16[512,128]{1,0:T(8,128)(2,1)}, u32[]{:S(2)}) copy-start(bf16[512,128]{1,0:T(8,128)(2,1)} %param.25) | copy-start | bytes 393220
  6.6 73.7 %all-gather.17.cloned.1.call-start = ((), (), s32[]{:S(2)}) async-start(), calls=%async_computation.6 | async-start | bytes 1572864 | tf_op jit(solution)/shard_map/all_gather | solution.py:124
  7.3 91.5 %all-gather.11.cloned.1.call-start = ((), (), s32[]{:S(2)}) async-start(), calls=%async_computation.2 | async-start | bytes 2621440 | tf_op jit(solution)/shard_map/all_gather | solution.py:137
  8.0 136.1 %all-gather.15.cloned.1.call-start = ((), (), s32[]{:S(2)}) async-start(), calls=%async_computation.4 | async-start | bytes 2621440 | tf_op jit(solution)/shard_map/all_gather | solution.py:136
  8.8 65.9 %copy-start.10 = (bf16[512,512]{1,0:T(8,128)(2,1)S(1)}, bf16[512,512]{1,0:T(8,128)(2,1)}, u32[]{:S(2)}) copy-start(bf16[512,512]{1,0:T(8,128)(2,1)} %param.23) | copy-start | bytes 1572868
  8.8 180.5 %all-gather.13.cloned.1.call-start = ((), (), s32[]{:S(2)}) async-start(), calls=%async_computation.3 | async-start | bytes 2621440 | tf_op jit(solution)/shard_map/all_gather | solution.py:138
  8.8 69.4 %collective-permute-start.2 = (bf16[512,512]{1,0:T(8,128)(2,1)}, bf16[512,512]{1,0:T(8,128)(2,1)}, u32[]{:S(2)}, u32[]{:S(2)}) collective-permute-start(bf16[512,512]{1,0:T(8,128)(2,1)} %param.23), channel_id=1, source_target_pairs={{0,8},{8,16},{16,24},{24,0},{1,9},{9,17},{17,25},{25,1},{2,10},{10... | collective-permute-start | bytes 1572872 | tf_op jit(solution)/shard_map/ppermute | solution.py:24
  12.0 220.7 %all-gather.19.cloned.1.call-start = ((), (), s32[]{:S(2)}) async-start(), calls=%async_computation.7 | async-start | bytes 1310720 | tf_op jit(solution)/shard_map/all_gather | solution.py:31
  78.3 17.6 %collective-permute-start.3 = (bf16[512,512]{1,0:T(8,128)(2,1)}, bf16[512,512]{1,0:T(8,128)(2,1)}, u32[]{:S(2)}, u32[]{:S(2)}) collective-permute-start(bf16[512,512]{1,0:T(8,128)(2,1)} %collective-permute-done.2), channel_id=1, source_target_pairs={{0,8},{8,16},{16,24},{24,0},{1,9},{9,17},{17,25},{25,1},{2,10},{10... | collective-permute-start | bytes 1572872 | tf_op jit(solution)/shard_map/ppermute | solution.py:24
  81.8 107.5 %copy-start.28 = (f32[256]{0:T(256)}, f32[256]{0:T(256)S(1)}, u32[]{:S(2)}) copy-start(f32[256]{0:T(256)S(1)} %add_rsqrt_fusion.1) | copy-start | bytes 3076
  84.3 14.5 %copy-start.31 = (f32[2048]{0:T(1024)S(1)}, f32[2048]{0:T(1024)}, u32[]{:S(2)}) copy-start(f32[2048]{0:T(1024)} %param.19) | copy-start | bytes 24580
  85.9 12.9 %copy-start.12 = (bf16[256,128]{1,0:T(8,128)(2,1)}, bf16[256,128]{1,0:T(8,128)(2,1)S(1)}, u32[]{:S(2)}) copy-start(bf16[256,128]{1,0:T(8,128)(2,1)S(1)} %convolution_convert_fusion.6) | copy-start | bytes 196612
  86.6 119.4 %collective-permute-start.1 = (bf16[128,128]{1,0:T(8,128)(2,1)}, bf16[128,128]{1,0:T(8,128)(2,1)}, u32[]{:S(2)}, u32[]{:S(2)}) collective-permute-start(bf16[128,128]{1,0:T(8,128)(2,1)} %slice.64), channel_id=1, source_target_pairs={{0,8},{8,16},{16,24},{1,9},{9,17},{17,25},{2,10},{10,18},{18,26},{... | collective-permute-start | bytes 98312 | tf_op jit(solution)/shard_map/ppermute | solution.py:54
  91.5 115.5 %collective-permute-start = (bf16[128,128]{1,0:T(8,128)(2,1)}, bf16[128,128]{1,0:T(8,128)(2,1)}, u32[]{:S(2)}, u32[]{:S(2)}) collective-permute-start(bf16[128,128]{1,0:T(8,128)(2,1)} %slice.63), channel_id=1, source_target_pairs={{0,8},{8,16},{16,24},{1,9},{9,17},{17,25},{2,10},{10,18},{18,26},{... | collective-permute-start | bytes 98312 | tf_op jit(solution)/shard_map/ppermute | solution.py:54
  95.8 112.1 %collective-permute-start.4 = (bf16[512,512]{1,0:T(8,128)(2,1)}, bf16[512,512]{1,0:T(8,128)(2,1)}, u32[]{:S(2)}, u32[]{:S(2)}) collective-permute-start(bf16[512,512]{1,0:T(8,128)(2,1)} %collective-permute-done.3), channel_id=1, source_target_pairs={{0,8},{8,16},{16,24},{24,0},{1,9},{9,17},{17,25},{25,1},{2,10},{10... | collective-permute-start | bytes 1572872 | tf_op jit(solution)/shard_map/ppermute | solution.py:24
  98.8 45.3 %copy-start.32 = (f32[2048]{0:T(1024)S(1)}, f32[2048]{0:T(1024)}, u32[]{:S(2)}) copy-start(f32[2048]{0:T(1024)} %param.19) | copy-start | bytes 24580
  196.0 11.0 %copy-start.13 = (bf16[256,128]{1,0:T(8,128)(2,1)S(1)}, bf16[256,128]{1,0:T(8,128)(2,1)}, u32[]{:S(2)}) copy-start(bf16[256,128]{1,0:T(8,128)(2,1)} %copy-done.12) | copy-start | bytes 196612
  205.7 68.6 %all-gather.21.cloned.1.call-start = ((), (), s32[]{:S(2)}) async-start(), calls=%async_computation.8 | async-start | bytes 2621440 | tf_op jit(solution)/shard_map/all_gather | solution.py:222
  214.0 18.7 %copy-start.22 = (f32[2]{0:T(128)S(1)}, f32[2]{0:T(128)}, u32[]{:S(2)}) copy-start(f32[2]{0:T(128)} %custom-call.1) | copy-start | bytes 28
  214.0 18.7 %copy-start.25 = (bf16[4,2]{1,0:T(4,128)(2,1)S(1)}, bf16[4,2]{1,0:T(4,128)(2,1)}, u32[]{:S(2)}) copy-start(bf16[4,2]{1,0:T(4,128)(2,1)} %reshape.302) | copy-start | bytes 52
  239.7 65.2 %reduce-scatter.2.cloned.1.call-start = ((), (), s32[]{:S(2)}) async-start(), calls=%async_computation.5 | async-start | bytes 1572864 | tf_op jit(solution)/shard_map/reduce_scatter | solution.py:231
  (25 other events, 84.2 us)
Sparse Core Ops, SparseCore 0:
  8.9 11.7 all-gather.16
  22.3 65.8 all-gather.10
  89.8 54.3 all-gather.14
  145.6 43.6 all-gather.12
  205.9 26.7 all-gather.18
  239.8 34.4 all-gather.20
  297.1 7.8 reduce-scatter.1
